TPU v7x, 32 devices: a whole 2x2x4 slice. The times are simulated.
32 devices in a mesh: sp: 16 (over z, y, x), tp: 2 (over core).
Axes of the slice: x: 2, y: 2, z: 4, core: 2. Of those that a mesh axis runs over, the one named last changes fastest.
Arguments:
- mixer_in: bfloat16 [8192, 1024], P('sp', 'tp'), may hold values from -6 to 6
- residual: bfloat16 [8192, 2048], P(('sp', 'tp')), may hold values from -6 to 6
- decay_real: float32 [64, 64], P('tp'), may hold values from -2 to 0, as said below
- decay_imag: float32 [64, 64], P('tp'), may hold values from 1 to 200
- log_step: float32 [64], P('tp'), may hold values from -3.9 to -2.5
- in_real: float32 [64, 64, 16], P('tp'), may hold values from -1 to 1
- in_imag: float32 [64, 64, 16], P('tp'), may hold values from -1 to 1
- output_real: float32 [64, 16, 64], P('tp'), may hold values from -0.5 to 0.5
- output_imaginary: float32 [64, 16, 64], P('tp'), may hold values from -0.5 to 0.5
- skip: float32 [1024], P('tp'), may hold values from -4 to 4
- out_proj: bfloat16 [1024, 2048], P('tp'), may hold values from -0.1875 to 0.1875
- norm_gain: float32 [2048], replicated, may hold values from 0.1 to 1.9
- w_gate: bfloat16 [2048, 5632], P('sp', 'tp'), may hold values from -0.125 to 0.125
- w_up: bfloat16 [2048, 5632], P('sp', 'tp'), may hold values from -0.125 to 0.125
- w_down: bfloat16 [5632, 2048], P('tp', 'sp'), may hold values from -0.078125 to 0.078125
Outputs:
- output: bfloat16 [8192, 2048], P(('sp', 'tp'))
Inputs may be any that keep to these rules, and one draw needn't show every extreme that they name: `decay_real`: every entry is negative.
All inputs are finite; a program needn't handle non-finite values.
Results may differ from a plain program's by a relative error of at most 0.02.
Values may be sent and summed in bfloat16 or wider, within the bound.
A program may use at most 128 MiB of HBM per device.

v0:
```python
import jax
import jax.numpy as jnp
from jax import lax
from jax.sharding import PartitionSpec as P


def prefix(value, axis, join, neutral):
    count, mine = (lax.axis_size(axis), lax.axis_index(axis))
    pieces = jax.tree.map(lambda part: lax.all_gather(part, axis), value)
    subtotal = jax.tree.map(
        lambda part, zero: jnp.full_like(part, 0) + jnp.asarray(zero, part.dtype), value, neutral
    )

    def step(position, subtotal):
        longer = join(subtotal, jax.tree.map(lambda part: part[position], pieces))
        return jax.tree.map(lambda new, old: jnp.where(position < mine, new, old), longer, subtotal)

    return lax.fori_loop(0, count - 1, step, subtotal)


def discrete(decay_real, decay_imag, log_step, in_real, in_imag):
    step_size = jnp.exp(log_step)[:, None]
    magnitude = jnp.exp(decay_real * step_size)
    angle = decay_imag * step_size
    power_re = magnitude * jnp.cos(angle)
    power_im = magnitude * jnp.sin(angle)
    denom = decay_real * decay_real + decay_imag * decay_imag
    ratio_re = ((power_re - 1.0) * decay_real + power_im * decay_imag) / denom
    ratio_im = (power_im * decay_real - (power_re - 1.0) * decay_imag) / denom
    drive_re = ratio_re[..., None] * in_real - ratio_im[..., None] * in_imag
    drive_im = ratio_re[..., None] * in_imag + ratio_im[..., None] * in_real
    return (power_re, power_im, drive_re, drive_im)


def combine(earlier, later):
    ar1, ai1, br1, bi1 = earlier
    ar2, ai2, br2, bi2 = later
    return (
        ar2 * ar1 - ai2 * ai1,
        ar2 * ai1 + ai2 * ar1,
        ar2 * br1 - ai2 * bi1 + br2,
        ar2 * bi1 + ai2 * br1 + bi2,
    )


def spread_blocks(matrix):
    groups = matrix.shape[0]
    unit_blocks = jnp.eye(groups, dtype=jnp.float32)[:, None, :, None]
    turned = jnp.transpose(matrix, (0, 2, 1))[:, :, None, :]
    return (unit_blocks * turned).reshape(groups * matrix.shape[2], groups * matrix.shape[1])


def local_states(power_re, power_im, drive_re, drive_im):
    rows, flat_size = drive_re.shape
    span = 8
    blocks = rows // span
    dr = drive_re.reshape(blocks, span, flat_size)
    di = drive_im.reshape(blocks, span, flat_size)
    cur_re = dr[:, 0]
    cur_im = di[:, 0]
    inner_re = [cur_re]
    inner_im = [cur_im]
    lift_re = [power_re]
    lift_im = [power_im]
    for index in range(1, span):
        cur_re, cur_im = (
            power_re * cur_re - power_im * cur_im + dr[:, index],
            power_re * cur_im + power_im * cur_re + di[:, index],
        )
        inner_re.append(cur_re)
        inner_im.append(cur_im)
        prev_re, prev_im = (lift_re[-1], lift_im[-1])
        lift_re.append(power_re * prev_re - power_im * prev_im)
        lift_im.append(power_re * prev_im + power_im * prev_re)
    inner_re = jnp.stack(inner_re, axis=1)
    inner_im = jnp.stack(inner_im, axis=1)
    lift_re = jnp.concatenate(lift_re, axis=0)[None]
    lift_im = jnp.concatenate(lift_im, axis=0)[None]
    block_re = jnp.broadcast_to(lift_re[0, span - 1][None], (blocks, flat_size))
    block_im = jnp.broadcast_to(lift_im[0, span - 1][None], (blocks, flat_size))
    totals = (block_re, block_im, cur_re, cur_im)
    distance = 1
    while distance < blocks:
        ones = jnp.ones((distance, flat_size), jnp.float32)
        zeros = jnp.zeros((distance, flat_size), jnp.float32)
        moved = (
            jnp.concatenate([ones, totals[0][:-distance]], axis=0),
            jnp.concatenate([zeros, totals[1][:-distance]], axis=0),
            jnp.concatenate([zeros, totals[2][:-distance]], axis=0),
            jnp.concatenate([zeros, totals[3][:-distance]], axis=0),
        )
        totals = combine(moved, totals)
        distance = distance * 2
    one_row = jnp.ones((1, flat_size), jnp.float32)
    zero_row = jnp.zeros((1, flat_size), jnp.float32)
    before_a_re = jnp.concatenate([one_row, totals[0][:-1]], axis=0)[:, None]
    before_a_im = jnp.concatenate([zero_row, totals[1][:-1]], axis=0)[:, None]
    before_re = jnp.concatenate([zero_row, totals[2][:-1]], axis=0)[:, None]
    before_im = jnp.concatenate([zero_row, totals[3][:-1]], axis=0)[:, None]
    state_real = inner_re + lift_re * before_re - lift_im * before_im
    state_imaginary = inner_im + lift_re * before_im + lift_im * before_re
    pw_re = lift_re * before_a_re - lift_im * before_a_im
    pw_im = lift_re * before_a_im + lift_im * before_a_re
    summary = (totals[0][-1], totals[1][-1], totals[2][-1], totals[3][-1])
    return (
        pw_re.reshape(rows, flat_size),
        pw_im.reshape(rows, flat_size),
        state_real.reshape(rows, flat_size),
        state_imaginary.reshape(rows, flat_size),
        summary,
    )


def on_device(
    mixer_in,
    residual,
    decay_real,
    decay_imag,
    log_step,
    in_real,
    in_imag,
    output_real,
    output_imaginary,
    skip,
    out_proj,
    norm_gain,
    w_gate,
    w_up,
    w_down,
):
    highest_precision = lax.Precision.HIGHEST
    power_re, power_im, bar_re, bar_im = discrete(
        decay_real, decay_imag, log_step, in_real, in_imag
    )
    flat_size = decay_real.shape[0] * decay_real.shape[1]
    read_in = jnp.concatenate([spread_blocks(bar_re), spread_blocks(bar_im)], axis=1)
    signal = mixer_in.astype(jnp.float32)
    drive = jnp.dot(signal, read_in, precision=highest_precision)
    drive_re = drive[:, :flat_size]
    drive_im = drive[:, flat_size:]
    pw_re, pw_im, state_real, state_imaginary, summary = local_states(
        power_re.reshape(1, flat_size), power_im.reshape(1, flat_size), drive_re, drive_im
    )
    zero_line = jnp.zeros((flat_size,), jnp.float32)
    identity = (jnp.ones((flat_size,), jnp.float32), zero_line, zero_line, zero_line)
    _, _, hold_re, hold_im = prefix(summary, "sp", combine, identity)
    state_real = state_real + pw_re * hold_re[None] - pw_im * hold_im[None]
    state_imaginary = state_imaginary + pw_re * hold_im[None] + pw_im * hold_re[None]
    read_out = jnp.concatenate(
        [spread_blocks(output_real), -spread_blocks(output_imaginary)], axis=0
    )
    mixed_before_norm = jnp.dot(
        jnp.concatenate([state_real, state_imaginary], axis=1),
        read_out,
        precision=highest_precision,
    )
    mixed_before_norm = mixed_before_norm + skip[None] * signal
    activated = jax.nn.gelu(mixed_before_norm).astype(jnp.bfloat16)
    partial_value = jnp.dot(activated, out_proj, preferred_element_type=jnp.float32).astype(
        jnp.bfloat16
    )
    mixed = lax.psum_scatter(
        lax.optimization_barrier(partial_value).astype(jnp.float32).astype(jnp.bfloat16),
        "tp",
        scatter_dimension=0,
        tiled=True,
    )
    carried = residual.astype(jnp.float32) + mixed.astype(jnp.float32)
    scale = lax.rsqrt(jnp.mean(carried * carried, axis=-1, keepdims=True) + 1e-06)
    normed = (carried * scale * norm_gain).astype(jnp.bfloat16)
    full_rows = lax.all_gather(normed, "tp", axis=0, tiled=True)
    gate = jnp.dot(
        full_rows,
        lax.all_gather(w_gate, "sp", axis=0, tiled=True),
        preferred_element_type=jnp.float32,
    )
    up = jnp.dot(
        full_rows,
        lax.all_gather(w_up, "sp", axis=0, tiled=True),
        preferred_element_type=jnp.float32,
    )
    down_columns = lax.all_gather(w_down, "sp", axis=1, tiled=True)
    hidden = (jax.nn.silu(gate) * up).astype(jnp.bfloat16)
    partial_value = jnp.dot(hidden, down_columns, preferred_element_type=jnp.float32).astype(
        jnp.bfloat16
    )
    down = lax.psum_scatter(
        lax.optimization_barrier(partial_value).astype(jnp.float32).astype(jnp.bfloat16),
        "tp",
        scatter_dimension=0,
        tiled=True,
    )
    return (carried + 0.5 * down.astype(jnp.float32)).astype(jnp.bfloat16)


def solution(mesh):
    return jax.shard_map(
        on_device,
        mesh=mesh,
        in_specs=(
            P("sp", "tp"),
            P(("sp", "tp"), None),
            P("tp", None),
            P("tp", None),
            P("tp"),
            P("tp", None, None),
            P("tp", None, None),
            P("tp", None, None),
            P("tp", None, None),
            P("tp"),
            P("tp", None),
            P(),
            P("sp", "tp"),
            P("sp", "tp"),
            P("tp", "sp"),
        ),
        out_specs=P(("sp", "tp"), None),
        check_vma=False,
    )
```

profile of v0, /device:TPU:0, one launch (start us, length us, event | category | flops | bytes accessed | tf_op | source)
XLA Modules:
  0.0 897.7 jit_solution(369592521946466958)
XLA Ops:
  9.7 8.3 broadcast_multiply_fusion.2
  18.1 7.8 mul.1865
  25.9 7.9 mul.1870
  33.8 10.5 %fusion.11 = f32[512,4096]{1,0:T(8,128)S(1)} fusion(bf16[512,512]{1,0:T(8,128)(2,1)S(1)} %copy-done.39, f32[512,2048]{1,0:T(8,128)} %mul.1870, f32[512,2048]{1,0:T(8,128)} %mul.1865), kind=kOutput, calls=%fused_computation.18 | convolution fusion | flops 12886999040 | bytes 17301504 | tf_op jit(solution)/shard_map/dot_general | solution.py:138
  89.2 43.1 %all-gather.2 = f32[16,1,2048]{2,1,0:T(1,128)S(1)} all-gather(f32[1,1,2048]{2,1,0:T(1,128)S(1)} %slice_bitcast_fusion.3), channel_id=1, replica_groups=mesh['sp'=16,'tp'=2] {'sp'}, dimensions={0}, use_global_device_ids=true | all-gather | bytes 139264 | tf_op jit(solution)/shard_map/all_gather | solution.py:9
  132.3 36.1 %all-gather.1 = f32[16,1,2048]{2,1,0:T(1,128)S(1)} all-gather(f32[1,1,2048]{2,1,0:T(1,128)S(1)} %slice_bitcast_fusion.4), channel_id=1, replica_groups=mesh['sp'=16,'tp'=2] {'sp'}, dimensions={0}, use_global_device_ids=true | all-gather | bytes 139264 | tf_op jit(solution)/shard_map/all_gather | solution.py:9
  168.5 38.2 %all-gather = f32[16,1,2048]{2,1,0:T(1,128)S(1)} all-gather(f32[1,1,2048]{2,1,0:T(1,128)S(1)} %slice_bitcast_fusion.5), channel_id=1, replica_groups=mesh['sp'=16,'tp'=2] {'sp'}, dimensions={0}, use_global_device_ids=true | all-gather | bytes 139264 | tf_op jit(solution)/shard_map/all_gather | solution.py:9
  207.5 36.2 %all-gather.3 = f32[16,1,2048]{2,1,0:T(1,128)S(1)} all-gather(f32[1,1,2048]{2,1,0:T(1,128)S(1)} %slice_bitcast_fusion.2), channel_id=1, replica_groups=mesh['sp'=16,'tp'=2] {'sp'}, dimensions={0}, use_global_device_ids=true | all-gather | bytes 139264 | tf_op jit(solution)/shard_map/all_gather | solution.py:9
  244.3 26.6 %while.16 = (s32[]{:T(128)}, f32[2048]{0:T(1024)S(1)}, f32[2048]{0:T(1024)S(1)}, s32[]{:T(128)}, f32[16,2048]{1,0:T(8,128)}, /*index=5*/f32[16,2048]{1,0:T(8,128...) while((s32[]{:T(128)}, f32[2048]{0:T(1024)S(1)}, f32[2048]{0:T(1024)S(1)}, ...), condition=%wide.region_1.2_spmd.clone, body=%wide.region_0.1_spmd.clone.sunk | while | flops 24580 | bytes 131201 | solution.py:18
  284.8 8.1 broadcast_multiply_fusion
  293.0 7.8 mul.2031
  300.8 7.8 neg.11
  310.5 11.9 %stack.5 = f32[64,8,2048]{2,1,0:T(8,128)} concatenate(f32[64,1,2048]{2,1,0:T(1,128)S(1)} %get-tuple-element.246, f32[64,1,2048]{2,1,0:T(1,128)} %copy.106, f32[64,1,2048]{2,1,0:T(1,128)} %copy.107, f32[64,1,2048]{2,1,0:T(1,128)} %copy.108, f32[64,1,2048]{2,1,0:T(1,128)} %copy.109, f32[64,1,2048]{2,1,0:T(1,128)} %copy.110, f32[64,1,2048]{2,1,0:T(1,128)} %copy.111, ...), dimensions={1} | concatenate | bytes 8388608 | tf_op jit(solution)/shard_map/stack | solution.py:76
  322.4 12.0 %stack.4 = f32[64,8,2048]{2,1,0:T(8,128)} concatenate(f32[64,1,2048]{2,1,0:T(1,128)S(1)} %get-tuple-element.248, f32[64,1,2048]{2,1,0:T(1,128)} %copy.98, f32[64,1,2048]{2,1,0:T(1,128)} %copy.99, f32[64,1,2048]{2,1,0:T(1,128)} %copy.100, f32[64,1,2048]{2,1,0:T(1,128)} %copy.101, f32[64,1,2048]{2,1,0:T(1,128)} %copy.102, f32[64,1,2048]{2,1,0:T(1,128)} %copy.103, ...), dimensions={1} | concatenate | bytes 8388608 | tf_op jit(solution)/shard_map/stack | solution.py:75
  334.4 7.0 fusion.15
  342.3 16.5 %fusion.24 = bf16[512,512]{1,0:T(8,128)(2,1)S(1)} fusion(bf16[512,512]{1,0:T(8,128)(2,1)S(1)} %copy-done.40, f32[2048,512]{0,1:T(8,128)S(1)} %copy-done.22, f32[2048,512]{0,1:T(8,128)S(1)} %copy-done.21, f32[512,2048]{1,0:T(8,128)} %get-tuple-element.258, f32[512,2048]{1,0:T(8,128)S(1)} %get-tuple-element.257, f32[512]{0:T(512)S(1)} %copy-done.50), kind=kOutput, calls=%fused_computation.49 | convolution fusion | flops 12892241920 | bytes 17827840 | tf_op jit(solution)/shard_map/dot_general | solution.py:152
  361.5 7.6 reduce-scatter.3.cloned.1.call-done
  375.3 10.1 %all-gather.9.cloned.1.call-done = bf16[512,2048]{1,0:T(8,128)(2,1)} async-done(((bf16[256,2048]{1,0:T(8,128)(2,1)}), bf16[512,2048]{1,0:T(8,128)(2,1)}) %all-gather.9.cloned.1.call-update) | async-done | bytes 2097168 | tf_op jit(solution)/shard_map/all_gather | solution.py:171
  385.4 145.4 %all-gather.11.cloned.1.call-done = bf16[2048,2816]{1,0:T(8,128)(2,1)} async-done(((bf16[128,2816]{1,0:T(8,128)(2,1)}), bf16[2048,2816]{1,0:T(8,128)(2,1)}) %all-gather.11.cloned.1.call-update) | async-done | bytes 11534352 | tf_op jit(solution)/shard_map/all_gather | solution.py:174
  530.8 12.7 %fusion.63 = f32[512,2816]{1,0:T(8,128)} fusion(bf16[512,2048]{1,0:T(8,128)(2,1)} %all-gather.9.cloned.1.call-done, bf16[2048,2816]{1,0:T(8,128)(2,1)} %all-gather.11.cloned.1.call-done), kind=kOutput, calls=%fused_computation.183 | convolution fusion | flops 5905580032 | bytes 19398656 | tf_op jit(solution)/shard_map/dot_general | solution.py:172
  543.5 129.6 %all-gather.13.cloned.1.call-done = bf16[2048,2816]{1,0:T(8,128)(2,1)} async-done(((bf16[128,2816]{1,0:T(8,128)(2,1)}), bf16[2048,2816]{1,0:T(8,128)(2,1)}) %all-gather.13.cloned.1.call-update) | async-done | bytes 11534352 | tf_op jit(solution)/shard_map/all_gather | solution.py:179
  673.0 182.8 %all-gather.15.cloned.1.call-done = bf16[2816,2048]{1,0:T(8,128)(2,1)} async-done(((bf16[2816,128]{1,0:T(8,128)(2,1)}), bf16[2816,2048]{1,0:T(8,128)(2,1)}) %all-gather.15.cloned.1.call-update) | async-done | bytes 11534352 | tf_op jit(solution)/shard_map/all_gather | solution.py:182
  855.8 23.4 %convolution_convert_fusion = bf16[512,2048]{1,0:T(8,128)(2,1)} fusion(bf16[2816,2048]{1,0:T(8,128)(2,1)} %all-gather.15.cloned.1.call-done, f32[512,2816]{1,0:T(8,128)} %fusion.63, bf16[512,2048]{1,0:T(8,128)(2,1)} %all-gather.9.cloned.1.call-done, bf16[2048,2816]{1,0:T(8,128)(2,1)} %all-gather.13.cloned.1.call-done), kind=kOutput, calls=%fused_computation.35 | convolution fusion | flops 11820859392 | bytes 33030144 | tf_op jit(solution)/shard_map/dot_general | solution.py:184
  879.2 8.1 reduce-scatter.5.cloned.1.call-done
  (240 shorter events, 103.5 us)
Async XLA Ops:
  6.5 352.3 %copy-start = (bf16[512,2048]{1,0:T(8,128)(2,1)S(1)}, bf16[512,2048]{1,0:T(8,128)(2,1)}, u32[]{:S(2)}) copy-start(bf16[512,2048]{1,0:T(8,128)(2,1)} %param.27) | copy-start | bytes 6291460
  6.5 362.6 %reduce-scatter.3.cloned.1.call-start = ((), (), s32[]{:S(2)}) async-start(), calls=%async_computation.2 | async-start | bytes 3145728 | tf_op jit(solution)/shard_map/reduce_scatter | solution.py:162
  6.5 11.5 %copy-start.47 = (f32[32,32]{0,1:T(8,128)}, f32[32,32]{0,1:T(8,128)S(1)}, u32[]{:S(2)}) copy-start(f32[32,32]{0,1:T(8,128)S(1)} %fusion.52) | copy-start | bytes 12292
  76.0 12.5 %copy-start.24 = (f32[64,2048]{1,0:T(8,128)S(1)}, f32[64,2048]{1,0:T(8,128)}, u32[]{:S(2)}) copy-start(f32[64,2048]{1,0:T(8,128)} %fusion.38) | copy-start | bytes 1572868
  76.0 12.5 %copy-start.23 = (f32[64,2048]{1,0:T(8,128)S(1)}, f32[64,2048]{1,0:T(8,128)}, u32[]{:S(2)}) copy-start(f32[64,2048]{1,0:T(8,128)} %get-tuple-element.206) | copy-start | bytes 1572868
  76.0 12.5 %copy-start.9 = (f32[64,2048]{1,0:T(8,128)S(1)}, f32[64,2048]{1,0:T(8,128)}, u32[]{:S(2)}) copy-start(f32[64,2048]{1,0:T(8,128)} %copy-done.8) | copy-start | bytes 1572868
  76.0 12.5 %copy-start.11 = (f32[64,2048]{1,0:T(8,128)S(1)}, f32[64,2048]{1,0:T(8,128)}, u32[]{:S(2)}) copy-start(f32[64,2048]{1,0:T(8,128)} %copy-done.10) | copy-start | bytes 1572868
  76.0 12.5 %copy-start.38 = (f32[48,2048]{1,0:T(8,128)S(1)}, f32[48,2048]{1,0:T(8,128)}, u32[]{:S(2)}) copy-start(f32[48,2048]{1,0:T(8,128)} %slice.234) | copy-start | bytes 1179652
  88.8 118.6 %copy-start.25 = (f32[64,2048]{1,0:T(8,128)}, f32[64,2048]{1,0:T(8,128)S(1)}, u32[]{:S(2)}) copy-start(f32[64,2048]{1,0:T(8,128)S(1)} %get-tuple-element.203) | copy-start | bytes 1572868
  89.1 118.3 %copy-start.26 = (f32[64,2048]{1,0:T(8,128)}, f32[64,2048]{1,0:T(8,128)S(1)}, u32[]{:S(2)}) copy-start(f32[64,2048]{1,0:T(8,128)S(1)} %get-tuple-element.262) | copy-start | bytes 1572868
  89.1 154.5 %copy-start.27 = (f32[64,2048]{1,0:T(8,128)}, f32[64,2048]{1,0:T(8,128)S(1)}, u32[]{:S(2)}) copy-start(f32[64,2048]{1,0:T(8,128)S(1)} %get-tuple-element.261) | copy-start | bytes 1572868
  89.1 154.5 %copy-start.28 = (f32[64,2048]{1,0:T(8,128)}, f32[64,2048]{1,0:T(8,128)S(1)}, u32[]{:S(2)}) copy-start(f32[64,2048]{1,0:T(8,128)S(1)} %get-tuple-element.267) | copy-start | bytes 1572868
  271.0 12.3 %copy-start.31 = (f32[64,1,2048]{2,0,1:T(8,128)S(1)}, f32[64,1,2048]{2,0,1:T(8,128)}, u32[]{:S(2)}) copy-start(f32[64,1,2048]{2,0,1:T(8,128)} %get-tuple-element.199) | copy-start | bytes 1572868
  271.0 13.6 %copy-start.45 = (f32[32,16,64]{2,1,0:T(8,128)S(1)}, f32[32,16,64]{2,1,0:T(8,128)}, u32[]{:S(2)}) copy-start(f32[32,16,64]{2,1,0:T(8,128)} %param.24) | copy-start | bytes 393220
  273.0 11.7 %copy-start.46 = (f32[32,16,64]{2,1,0:T(8,128)S(1)}, f32[32,16,64]{2,1,0:T(8,128)}, u32[]{:S(2)}) copy-start(f32[32,16,64]{2,1,0:T(8,128)} %param.25) | copy-start | bytes 393220
  273.0 11.8 %copy-start.48 = (f32[32,32]{0,1:T(8,128)S(1)}, f32[32,32]{0,1:T(8,128)}, u32[]{:S(2)}) copy-start(f32[32,32]{0,1:T(8,128)} %copy-done.47) | copy-start | bytes 12292
  322.4 12.0 %copy-start.37 = (f32[64,2048]{1,0:T(8,128)S(1)}, f32[64,2048]{1,0:T(8,128)}, u32[]{:S(2)}) copy-start(f32[64,2048]{1,0:T(8,128)} %concatenate.124) | copy-start | bytes 1572868
  322.4 12.0 %copy-start.42 = (f32[8,2048]{1,0:T(8,128)S(1)}, f32[8,2048]{1,0:T(8,128)}, u32[]{:S(2)}) copy-start(f32[8,2048]{1,0:T(8,128)} %copy-done.41) | copy-start | bytes 196612
  322.4 12.0 %copy-start.44 = (f32[8,2048]{1,0:T(8,128)S(1)}, f32[8,2048]{1,0:T(8,128)}, u32[]{:S(2)}) copy-start(f32[8,2048]{1,0:T(8,128)} %copy-done.43) | copy-start | bytes 196612
  361.4 23.9 %all-gather.9.cloned.1.call-start = ((), (), s32[]{:S(2)}) async-start(), calls=%async_computation.3 | async-start | bytes 3145728 | tf_op jit(solution)/shard_map/all_gather | solution.py:171
  373.4 157.4 %all-gather.11.cloned.1.call-start = ((), (), s32[]{:S(2)}) async-start(), calls=%async_computation.4 | async-start | bytes 12255232 | tf_op jit(solution)/shard_map/all_gather | solution.py:174
  374.1 298.9 %all-gather.13.cloned.1.call-start = ((), (), s32[]{:S(2)}) async-start(), calls=%async_computation.5 | async-start | bytes 12255232 | tf_op jit(solution)/shard_map/all_gather | solution.py:179
  374.7 481.1 %all-gather.15.cloned.1.call-start = ((), (), s32[]{:S(2)}) async-start(), calls=%async_computation.6 | async-start | bytes 12255232 | tf_op jit(solution)/shard_map/all_gather | solution.py:182
  375.3 512.1 %reduce-scatter.5.cloned.1.call-start = ((), (), s32[]{:S(2)}) async-start(), calls=%async_computation.7 | async-start | bytes 3145728 | tf_op jit(solution)/shard_map/reduce_scatter | solution.py:187
  (33 other events, 230.0 us)
Sparse Core Ops, SparseCore 0:
  361.6 7.4 reduce-scatter.2
  373.5 11.8 all-gather.8
  388.1 142.5 all-gather.10
  533.4 139.5 all-gather.12
  675.6 180.2 all-gather.14
  879.3 7.9 reduce-scatter.4
where the time goes:
time: 910 us; the launch traced here: 898 us
  waiting for transfers between devices  485 us (53%)
  blocking collectives  154 us (17%)
  local copies, waits for them, and re-layouts  123 us (14%)
  matrix products  65.6 us (7%)
  other arithmetic  54.9 us (6%)
  between operations  14.7 us (2%)
    all_gather x1, waiting for transfers between devices, on_device(): down_columns = lax.all_gather(w_down, 'sp', axis=1, tiled=True)  183 us
    all_gather x4, blocking collectives, prefix(): pieces = jax.tree.map(lambda part: lax.all_gather(part, axis), value)  154 us
    all_gather x1, waiting for transfers between devices, on_device(): lax.all_gather(w_gate, 'sp', axis=0, tiled=True)  145 us
    all_gather x1, waiting for transfers between devices, on_device(): lax.all_gather(w_up, 'sp', axis=0, tiled=True)  130 us
    dynamic_slice x30, local copies, waits for them, and re-layouts, step(): longer = join(subtotal, jax.tree.map(lambda part: part[position], pieces))  25.8 us
    mul x3, local copies, waits for them, and re-layouts, spread_blocks(): unit_blocks * turned  23.5 us
    dot_general x1, matrix products, on_device(): jnp.dot(hidden, down_columns, preferred_element_type=jnp.float32)  23.4 us
  transfers between devices with their start and end apart: 6, of which 6 were waited for; matrix products, arithmetic and copies ran while one was open for 1% of the time, Pallas kernels for 0%

commit v1 on v0

--- a/solution.py
+++ b/solution.py
@@ -179,7 +179,30 @@
         lax.all_gather(w_up, "sp", axis=0, tiled=True),
         preferred_element_type=jnp.float32,
     )
-    down_columns = lax.all_gather(w_down, "sp", axis=1, tiled=True)
+    out_arr = lax.axis_size("sp")
+    block_now = lax.axis_index("sp")
+    current_block, v_now, z_new = (out_arr, block_now, w_down.shape[1])
+    line_up = [it * current_block if ix == 1 else it for ix, it in enumerate(w_down.shape)]
+    down_columns = lax.dynamic_update_slice_in_dim(
+        jnp.zeros(line_up, w_down.dtype), w_down, v_now * z_new, axis=1
+    )
+    local_part = extra = w_down
+    src_i = 1
+    while src_i < current_block // 2 + 1:
+        local_part = lax.ppermute(
+            local_part, "sp", [(ix, (ix + 1) % current_block) for ix in range(current_block)]
+        )
+        down_columns = lax.dynamic_update_slice_in_dim(
+            down_columns, local_part, (v_now - src_i) % current_block * z_new, axis=1
+        )
+        if 2 * src_i < current_block:
+            extra = lax.ppermute(
+                extra, "sp", [(ix, (ix - 1) % current_block) for ix in range(current_block)]
+            )
+            down_columns = lax.dynamic_update_slice_in_dim(
+                down_columns, extra, (v_now + src_i) % current_block * z_new, axis=1
+            )
+        src_i = src_i + 1
     hidden = (jax.nn.silu(gate) * up).astype(jnp.bfloat16)
     partial_value = jnp.dot(hidden, down_columns, preferred_element_type=jnp.float32).astype(
         jnp.bfloat16

time: 910 us -> 869 us (0.955)
  waiting for transfers between devices: 485 us -> 355 us
  starting transfers between devices: 0.2 us -> 51.3 us
  local copies, waits for them, and re-layouts: 123 us -> 159 us
    ppermute x0 -> x15, waiting for transfers between devices: none -> 230 us  [the longest x8 205 us: on_device(): lax.ppermute(local_part, 'sp', [(ix, (ix + 1) % current_block) for ix in...]
    all_gather x1 -> x0, waiting for transfers between devices: 183 us -> none  [on_device(): down_columns = lax.all_gather(w_down, 'sp', axis=1, tiled=True)]
    all_gather x1, waiting for transfers between devices: 145 us -> 0.01 us  [on_device(): lax.all_gather(w_gate, 'sp', axis=0, tiled=True)]
    ppermute x0 -> x15, starting transfers between devices: none -> 51.1 us  [the longest x7 32.6 us: on_device(): lax.ppermute(extra, 'sp', [(ix, (ix - 1) % current_block) for ix in range...]
    dynamic_update_slice x0 -> x16, local copies, waits for them, and re-layouts: none -> 23.9 us  [the longest x8 12.5 us: on_device(): lax.dynamic_update_slice_in_dim(down_columns, local_part, (v_now - src_i)...]
    all_gather x1, waiting for transfers between devices: 130 us -> 108 us  [on_device(): lax.all_gather(w_up, 'sp', axis=0, tiled=True)]
    all_gather x1, waiting for transfers between devices: 10.1 us -> 0.01 us  [on_device(): full_rows = lax.all_gather(normed, 'tp', axis=0, tiled=True)]
  transfers between devices with their start and end apart: 6 -> 20, of which waited for: 6 -> 14; matrix products, arithmetic and copies ran while one was open for 1% -> 5% of each run, Pallas kernels for 0% -> 0%
where the time goes in v1:
time: 869 us; the launch traced here: 856 us
  waiting for transfers between devices  355 us (41%)
  local copies, waits for them, and re-layouts  159 us (18%)
  blocking collectives  154 us (18%)
  matrix products  65.3 us (8%)
  other arithmetic  57.2 us (7%)
  starting transfers between devices  51.3 us (6%)
  between operations  14.3 us (2%)
    ppermute x8, waiting for transfers between devices, on_device(): lax.ppermute(local_part, 'sp', [(ix, (ix + 1) % current_block) for ix in...  205 us
    all_gather x4, blocking collectives, prefix(): pieces = jax.tree.map(lambda part: lax.all_gather(part, axis), value)  154 us
    all_gather x1, waiting for transfers between devices, on_device(): lax.all_gather(w_up, 'sp', axis=0, tiled=True)  108 us
    ppermute x7, starting transfers between devices, on_device(): lax.ppermute(extra, 'sp', [(ix, (ix - 1) % current_block) for ix in range...  32.6 us
    dynamic_slice x30, local copies, waits for them, and re-layouts, step(): longer = join(subtotal, jax.tree.map(lambda part: part[position], pieces))  26.7 us
    ppermute x7, waiting for transfers between devices, on_device(): lax.ppermute(extra, 'sp', [(ix, (ix - 1) % current_block) for ix in range...  24.6 us
    mul x3, local copies, waits for them, and re-layouts, spread_blocks(): unit_blocks * turned  23.5 us
    dot_general x1, matrix products, on_device(): jnp.dot(hidden, down_columns, preferred_element_type=jnp.float32)  23.3 us
  transfers between devices with their start and end apart: 20, of which 14 were waited for; matrix products, arithmetic and copies ran while one was open for 5% of the time, Pallas kernels for 0%

profile of v1, /device:TPU:0, one launch (start us, length us, event | category | flops | bytes accessed | tf_op | source)
XLA Modules:
  0.0 856.2 jit_solution(8256501099513321165)
XLA Ops:
  9.7 8.3 broadcast_multiply_fusion.2
  33.8 10.5 %fusion.11 = f32[512,4096]{1,0:T(8,128)S(1)} fusion(bf16[512,512]{1,0:T(8,128)(2,1)S(1)} %copy-done.31, f32[512,2048]{1,0:T(8,128)} %mul.1918, f32[512,2048]{1,0:T(8,128)} %mul.1913), kind=kOutput, calls=%fused_computation.18 | convolution fusion | flops 12886999040 | bytes 17301504 | tf_op jit(solution)/shard_map/dot_general | solution.py:138
  92.6 43.2 %all-gather.2 = f32[16,1,2048]{2,1,0:T(1,128)S(1)} all-gather(f32[1,1,2048]{2,1,0:T(1,128)S(1)} %slice_bitcast_fusion.3), channel_id=1, replica_groups=mesh['sp'=16,'tp'=2] {'sp'}, dimensions={0}, use_global_device_ids=true | all-gather | bytes 139264 | tf_op jit(solution)/shard_map/all_gather | solution.py:9
  136.6 36.2 %all-gather.1 = f32[16,1,2048]{2,1,0:T(1,128)S(1)} all-gather(f32[1,1,2048]{2,1,0:T(1,128)S(1)} %slice_bitcast_fusion.4), channel_id=1, replica_groups=mesh['sp'=16,'tp'=2] {'sp'}, dimensions={0}, use_global_device_ids=true | all-gather | bytes 139264 | tf_op jit(solution)/shard_map/all_gather | solution.py:9
  173.5 38.1 %all-gather = f32[16,1,2048]{2,1,0:T(1,128)S(1)} all-gather(f32[1,1,2048]{2,1,0:T(1,128)S(1)} %slice_bitcast_fusion.5), channel_id=1, replica_groups=mesh['sp'=16,'tp'=2] {'sp'}, dimensions={0}, use_global_device_ids=true | all-gather | bytes 139264 | tf_op jit(solution)/shard_map/all_gather | solution.py:9
  212.4 36.3 %all-gather.3 = f32[16,1,2048]{2,1,0:T(1,128)S(1)} all-gather(f32[1,1,2048]{2,1,0:T(1,128)S(1)} %slice_bitcast_fusion.2), channel_id=1, replica_groups=mesh['sp'=16,'tp'=2] {'sp'}, dimensions={0}, use_global_device_ids=true | all-gather | bytes 139264 | tf_op jit(solution)/shard_map/all_gather | solution.py:9
  249.3 27.6 %while.16 = (s32[]{:T(128)}, f32[2048]{0:T(1024)S(1)}, f32[2048]{0:T(1024)S(1)}, s32[]{:T(128)}, f32[16,2048]{1,0:T(8,128)}, /*index=5*/f32[16,2048]{1,0:T(8,128...) while((s32[]{:T(128)}, f32[2048]{0:T(1024)S(1)}, f32[2048]{0:T(1024)S(1)}, ...), condition=%wide.region_1.2_spmd.clone, body=%wide.region_0.1_spmd.clone.sunk | while | flops 24580 | bytes 131201 | solution.py:18
  292.8 8.1 broadcast_multiply_fusion
  318.4 11.9 %stack.5 = f32[64,8,2048]{2,1,0:T(8,128)} concatenate(f32[64,1,2048]{2,1,0:T(1,128)S(1)} %get-tuple-element.246, f32[64,1,2048]{2,1,0:T(1,128)} %copy.106, f32[64,1,2048]{2,1,0:T(1,128)} %copy.107, f32[64,1,2048]{2,1,0:T(1,128)} %copy.108, f32[64,1,2048]{2,1,0:T(1,128)} %copy.109, f32[64,1,2048]{2,1,0:T(1,128)} %copy.110, f32[64,1,2048]{2,1,0:T(1,128)} %copy.111, ...), dimensions={1} | concatenate | bytes 8388608 | tf_op jit(solution)/shard_map/stack | solution.py:76
  330.4 12.0 %stack.4 = f32[64,8,2048]{2,1,0:T(8,128)} concatenate(f32[64,1,2048]{2,1,0:T(1,128)S(1)} %get-tuple-element.248, f32[64,1,2048]{2,1,0:T(1,128)} %copy.98, f32[64,1,2048]{2,1,0:T(1,128)} %copy.99, f32[64,1,2048]{2,1,0:T(1,128)} %copy.100, f32[64,1,2048]{2,1,0:T(1,128)} %copy.101, f32[64,1,2048]{2,1,0:T(1,128)} %copy.102, f32[64,1,2048]{2,1,0:T(1,128)} %copy.103, ...), dimensions={1} | concatenate | bytes 8388608 | tf_op jit(solution)/shard_map/stack | solution.py:75
  350.3 16.5 %fusion.24 = bf16[512,512]{1,0:T(8,128)(2,1)S(1)} fusion(bf16[512,512]{1,0:T(8,128)(2,1)S(1)} %copy-done.32, f32[2048,512]{0,1:T(8,128)S(1)} %copy-done.18, f32[2048,512]{0,1:T(8,128)S(1)} %copy-done.17, f32[512,2048]{1,0:T(8,128)} %get-tuple-element.258, f32[512,2048]{1,0:T(8,128)S(1)} %get-tuple-element.257, f32[512]{0:T(512)S(1)} %copy-done.42), kind=kOutput, calls=%fused_computation.49 | convolution fusion | flops 12892241920 | bytes 17827840 | tf_op jit(solution)/shard_map/dot_general | solution.py:152
  388.3 32.9 %collective-permute-done = bf16[2816,128]{1,0:T(8,128)(2,1)S(1)} collective-permute-done((bf16[2816,128]{1,0:T(8,128)(2,1)}, bf16[2816,128]{1,0:T(8,128)(2,1)S(1)}, u32[]{:S(2)}, u32[]{:S(2)}) %collective-permute-start) | collective-permute-done | bytes 720928 | tf_op jit(solution)/shard_map/ppermute | solution.py:192
  427.6 41.6 %collective-permute-done.2 = bf16[2816,128]{1,0:T(8,128)(2,1)} collective-permute-done((bf16[2816,128]{1,0:T(8,128)(2,1)S(1)}, bf16[2816,128]{1,0:T(8,128)(2,1)}, u32[]{:S(2)}, u32[]{:S(2)}) %collective-permute-start.2) | collective-permute-done | bytes 720928 | tf_op jit(solution)/shard_map/ppermute | solution.py:192
  475.3 10.6 %collective-permute-start.5 = (bf16[2816,128]{1,0:T(8,128)(2,1)}, bf16[2816,128]{1,0:T(8,128)(2,1)}, u32[]{:S(2)}, u32[]{:S(2)}) collective-permute-start(bf16[2816,128]{1,0:T(8,128)(2,1)} %collective-permute-done.3), channel_id=1, source_target_pairs={{0,30},{2,0},{4,2},{6,4},{8,6},{10,8},{12,10},{14,12},{16,14},{18,... | collective-permute-start | bytes 2162696 | tf_op jit(solution)/shard_map/ppermute | solution.py:199
  492.6 13.8 %collective-permute-done.4 = bf16[2816,128]{1,0:T(8,128)(2,1)} collective-permute-done((bf16[2816,128]{1,0:T(8,128)(2,1)}, bf16[2816,128]{1,0:T(8,128)(2,1)}, u32[]{:S(2)}, u32[]{:S(2)}) %collective-permute-start.4) | collective-permute-done | bytes 720928 | tf_op jit(solution)/shard_map/ppermute | solution.py:192
  516.2 38.0 %collective-permute-done.6 = bf16[2816,128]{1,0:T(8,128)(2,1)} collective-permute-done((bf16[2816,128]{1,0:T(8,128)(2,1)}, bf16[2816,128]{1,0:T(8,128)(2,1)}, u32[]{:S(2)}, u32[]{:S(2)}) %collective-permute-start.6) | collective-permute-done | bytes 720928 | tf_op jit(solution)/shard_map/ppermute | solution.py:192
  567.1 36.6 %collective-permute-done.8 = bf16[2816,128]{1,0:T(8,128)(2,1)S(1)} collective-permute-done((bf16[2816,128]{1,0:T(8,128)(2,1)}, bf16[2816,128]{1,0:T(8,128)(2,1)S(1)}, u32[]{:S(2)}, u32[]{:S(2)}) %collective-permute-start.8) | collective-permute-done | bytes 720928 | tf_op jit(solution)/shard_map/ppermute | solution.py:192
  614.6 30.1 %collective-permute-done.10 = bf16[2816,128]{1,0:T(8,128)(2,1)S(1)} collective-permute-done((bf16[2816,128]{1,0:T(8,128)(2,1)S(1)}, bf16[2816,128]{1,0:T(8,128)(2,1)S(1)}, u32[]{:S(2)}, u32[]{:S(2)}) %collective-permute-start.10) | collective-permute-done | bytes 720928 | tf_op jit(solution)/shard_map/ppermute | solution.py:192
  649.1 11.8 %collective-permute-start.13 = (bf16[2816,128]{1,0:T(8,128)(2,1)S(1)}, bf16[2816,128]{1,0:T(8,128)(2,1)S(1)}, u32[]{:S(2)}, u32[]{:S(2)}) collective-permute-start(bf16[2816,128]{1,0:T(8,128)(2,1)S(1)} %collective-permute-done.11), channel_id=1, source_target_pairs={{0,30},{2,0},{4,2},{6,4},{8,6},{10,8},{12,10},{14,12},{16,14},{18,... | collective-permute-start | bytes 2162696 | tf_op jit(solution)/shard_map/ppermute | solution.py:199
  665.6 13.9 %collective-permute-done.13 = bf16[2816,128]{1,0:T(8,128)(2,1)S(1)} collective-permute-done((bf16[2816,128]{1,0:T(8,128)(2,1)S(1)}, bf16[2816,128]{1,0:T(8,128)(2,1)S(1)}, u32[]{:S(2)}, u32[]{:S(2)}) %collective-permute-start.13) | collective-permute-done | bytes 720928 | tf_op jit(solution)/shard_map/ppermute | solution.py:199
  680.6 12.3 %collective-permute-done.14 = bf16[2816,128]{1,0:T(8,128)(2,1)S(1)} collective-permute-done((bf16[2816,128]{1,0:T(8,128)(2,1)S(1)}, bf16[2816,128]{1,0:T(8,128)(2,1)S(1)}, u32[]{:S(2)}, u32[]{:S(2)}) %collective-permute-start.14) | collective-permute-done | bytes 720928 | tf_op jit(solution)/shard_map/ppermute | solution.py:192
  694.0 12.5 %fusion.63 = f32[512,2816]{1,0:T(8,128)} fusion(bf16[512,2048]{1,0:T(8,128)(2,1)} %all-gather.8.cloned.1.call-done, bf16[2048,2816]{1,0:T(8,128)(2,1)} %all-gather.10.cloned.1.call-done), kind=kOutput, calls=%fused_computation.199 | convolution fusion | flops 5905580032 | bytes 19398656 | tf_op jit(solution)/shard_map/dot_general | solution.py:172
  706.4 108.3 %all-gather.12.cloned.1.call-done = bf16[2048,2816]{1,0:T(8,128)(2,1)} async-done(((bf16[128,2816]{1,0:T(8,128)(2,1)}), bf16[2048,2816]{1,0:T(8,128)(2,1)}) %all-gather.12.cloned.1.call-update) | async-done | bytes 11534352 | tf_op jit(solution)/shard_map/all_gather | solution.py:179
  814.8 23.3 %convolution_convert_fusion = bf16[512,2048]{1,0:T(8,128)(2,1)} fusion(bf16[2816,2048]{1,0:T(8,128)(2,1)} %constant_dynamic-update-slice_fusion, f32[512,2816]{1,0:T(8,128)} %fusion.63, bf16[512,2048]{1,0:T(8,128)(2,1)} %all-gather.8.cloned.1.call-done, bf16[2048,2816]{1,0:T(8,128)(2,1)} %all-gather.12.cloned.1.call-done), kind=kOutput, calls=%fused_computation.35 | convolution fusion | flops 11820859392 | bytes 33030144 | tf_op jit(solution)/shard_map/dot_general | solution.py:207
  (268 shorter events, 234.4 us)
Async XLA Ops:
  6.5 360.3 %copy-start = (bf16[512,2048]{1,0:T(8,128)(2,1)S(1)}, bf16[512,2048]{1,0:T(8,128)(2,1)}, u32[]{:S(2)}) copy-start(bf16[512,2048]{1,0:T(8,128)(2,1)} %param.27) | copy-start | bytes 6291460
  6.5 370.4 %reduce-scatter.3.cloned.1.call-start = ((), (), s32[]{:S(2)}) async-start(), calls=%async_computation.2 | async-start | bytes 3145728 | tf_op jit(solution)/shard_map/reduce_scatter | solution.py:162
  92.6 156.1 %copy-start.23 = (f32[64,2048]{1,0:T(8,128)}, f32[64,2048]{1,0:T(8,128)S(1)}, u32[]{:S(2)}) copy-start(f32[64,2048]{1,0:T(8,128)S(1)} %get-tuple-element.261) | copy-start | bytes 1572868
  92.6 156.1 %copy-start.24 = (f32[64,2048]{1,0:T(8,128)}, f32[64,2048]{1,0:T(8,128)S(1)}, u32[]{:S(2)}) copy-start(f32[64,2048]{1,0:T(8,128)S(1)} %get-tuple-element.267) | copy-start | bytes 1572868
  92.6 200.0 %copy-start.37 = (f32[32,16,64]{2,1,0:T(8,128)S(1)}, f32[32,16,64]{2,1,0:T(8,128)}, u32[]{:S(2)}) copy-start(f32[32,16,64]{2,1,0:T(8,128)} %param.24) | copy-start | bytes 393220
  369.4 324.5 %all-gather.8.cloned.1.call-start = ((), (), s32[]{:S(2)}) async-start(), calls=%async_computation.3 | async-start | bytes 3145728 | tf_op jit(solution)/shard_map/all_gather | solution.py:171
  381.3 312.7 %all-gather.10.cloned.1.call-start = ((), (), s32[]{:S(2)}) async-start(), calls=%async_computation.4 | async-start | bytes 12255232 | tf_op jit(solution)/shard_map/all_gather | solution.py:174
  382.0 432.8 %all-gather.12.cloned.1.call-start = ((), (), s32[]{:S(2)}) async-start(), calls=%async_computation.5 | async-start | bytes 12255232 | tf_op jit(solution)/shard_map/all_gather | solution.py:179
  382.6 463.6 %reduce-scatter.5.cloned.1.call-start = ((), (), s32[]{:S(2)}) async-start(), calls=%async_computation.6 | async-start | bytes 3145728 | tf_op jit(solution)/shard_map/reduce_scatter | solution.py:210
  382.6 38.5 %collective-permute-start = (bf16[2816,128]{1,0:T(8,128)(2,1)}, bf16[2816,128]{1,0:T(8,128)(2,1)S(1)}, u32[]{:S(2)}, u32[]{:S(2)}) collective-permute-start(bf16[2816,128]{1,0:T(8,128)(2,1)} %param.31), channel_id=1, source_target_pairs={{0,2},{2,4},{4,6},{6,8},{8,10},{10,12},{12,14},{14,16},{16,18},{18... | collective-permute-start | bytes 2162696 | tf_op jit(solution)/shard_map/ppermute | solution.py:192
  384.5 39.9 %collective-permute-start.1 = (bf16[2816,128]{1,0:T(8,128)(2,1)}, bf16[2816,128]{1,0:T(8,128)(2,1)}, u32[]{:S(2)}, u32[]{:S(2)}) collective-permute-start(bf16[2816,128]{1,0:T(8,128)(2,1)} %param.31), channel_id=1, source_target_pairs={{0,30},{2,0},{4,2},{6,4},{8,6},{10,8},{12,10},{14,12},{16,14},{18,... | collective-permute-start | bytes 2162696 | tf_op jit(solution)/shard_map/ppermute | solution.py:199
  422.0 47.2 %collective-permute-start.2 = (bf16[2816,128]{1,0:T(8,128)(2,1)S(1)}, bf16[2816,128]{1,0:T(8,128)(2,1)}, u32[]{:S(2)}, u32[]{:S(2)}) collective-permute-start(bf16[2816,128]{1,0:T(8,128)(2,1)S(1)} %collective-permute-done), channel_id=1, source_target_pairs={{0,2},{2,4},{4,6},{6,8},{8,10},{10,12},{12,14},{14,16},{16,18},{18... | collective-permute-start | bytes 2162696 | tf_op jit(solution)/shard_map/ppermute | solution.py:192
  424.4 50.9 %collective-permute-start.3 = (bf16[2816,128]{1,0:T(8,128)(2,1)}, bf16[2816,128]{1,0:T(8,128)(2,1)}, u32[]{:S(2)}, u32[]{:S(2)}) collective-permute-start(bf16[2816,128]{1,0:T(8,128)(2,1)} %collective-permute-done.1), channel_id=1, source_target_pairs={{0,30},{2,0},{4,2},{6,4},{8,6},{10,8},{12,10},{14,12},{16,14},{18,... | collective-permute-start | bytes 2162696 | tf_op jit(solution)/shard_map/ppermute | solution.py:199
  469.2 37.1 %collective-permute-start.4 = (bf16[2816,128]{1,0:T(8,128)(2,1)}, bf16[2816,128]{1,0:T(8,128)(2,1)}, u32[]{:S(2)}, u32[]{:S(2)}) collective-permute-start(bf16[2816,128]{1,0:T(8,128)(2,1)} %collective-permute-done.2), channel_id=1, source_target_pairs={{0,2},{2,4},{4,6},{6,8},{8,10},{10,12},{12,14},{14,16},{16,18},{18... | collective-permute-start | bytes 2162696 | tf_op jit(solution)/shard_map/ppermute | solution.py:192
  475.3 35.7 %collective-permute-start.5 = (bf16[2816,128]{1,0:T(8,128)(2,1)}, bf16[2816,128]{1,0:T(8,128)(2,1)}, u32[]{:S(2)}, u32[]{:S(2)}) collective-permute-start(bf16[2816,128]{1,0:T(8,128)(2,1)} %collective-permute-done.3), channel_id=1, source_target_pairs={{0,30},{2,0},{4,2},{6,4},{8,6},{10,8},{12,10},{14,12},{16,14},{18,... | collective-permute-start | bytes 2162696 | tf_op jit(solution)/shard_map/ppermute | solution.py:199
  506.3 47.8 %collective-permute-start.6 = (bf16[2816,128]{1,0:T(8,128)(2,1)}, bf16[2816,128]{1,0:T(8,128)(2,1)}, u32[]{:S(2)}, u32[]{:S(2)}) collective-permute-start(bf16[2816,128]{1,0:T(8,128)(2,1)} %collective-permute-done.4), channel_id=1, source_target_pairs={{0,2},{2,4},{4,6},{6,8},{8,10},{10,12},{12,14},{14,16},{16,18},{18... | collective-permute-start | bytes 2162696 | tf_op jit(solution)/shard_map/ppermute | solution.py:192
  511.0 54.0 %collective-permute-start.7 = (bf16[2816,128]{1,0:T(8,128)(2,1)}, bf16[2816,128]{1,0:T(8,128)(2,1)S(1)}, u32[]{:S(2)}, u32[]{:S(2)}) collective-permute-start(bf16[2816,128]{1,0:T(8,128)(2,1)} %collective-permute-done.5), channel_id=1, source_target_pairs={{0,30},{2,0},{4,2},{6,4},{8,6},{10,8},{12,10},{14,12},{16,14},{18,... | collective-permute-start | bytes 2162696 | tf_op jit(solution)/shard_map/ppermute | solution.py:199
  554.2 49.5 %collective-permute-start.8 = (bf16[2816,128]{1,0:T(8,128)(2,1)}, bf16[2816,128]{1,0:T(8,128)(2,1)S(1)}, u32[]{:S(2)}, u32[]{:S(2)}) collective-permute-start(bf16[2816,128]{1,0:T(8,128)(2,1)} %collective-permute-done.6), channel_id=1, source_target_pairs={{0,2},{2,4},{4,6},{6,8},{8,10},{10,12},{12,14},{14,16},{16,18},{18... | collective-permute-start | bytes 2162696 | tf_op jit(solution)/shard_map/ppermute | solution.py:192
  565.0 48.6 %collective-permute-start.9 = (bf16[2816,128]{1,0:T(8,128)(2,1)S(1)}, bf16[2816,128]{1,0:T(8,128)(2,1)S(1)}, u32[]{:S(2)}, u32[]{:S(2)}) collective-permute-start(bf16[2816,128]{1,0:T(8,128)(2,1)S(1)} %collective-permute-done.7), channel_id=1, source_target_pairs={{0,30},{2,0},{4,2},{6,4},{8,6},{10,8},{12,10},{14,12},{16,14},{18,... | collective-permute-start | bytes 2162696 | tf_op jit(solution)/shard_map/ppermute | solution.py:199
  603.7 41.0 %collective-permute-start.10 = (bf16[2816,128]{1,0:T(8,128)(2,1)S(1)}, bf16[2816,128]{1,0:T(8,128)(2,1)S(1)}, u32[]{:S(2)}, u32[]{:S(2)}) collective-permute-start(bf16[2816,128]{1,0:T(8,128)(2,1)S(1)} %collective-permute-done.8), channel_id=1, source_target_pairs={{0,2},{2,4},{4,6},{6,8},{8,10},{10,12},{12,14},{14,16},{16,18},{18... | collective-permute-start | bytes 2162696 | tf_op jit(solution)/shard_map/ppermute | solution.py:192
  613.6 35.5 %collective-permute-start.11 = (bf16[2816,128]{1,0:T(8,128)(2,1)S(1)}, bf16[2816,128]{1,0:T(8,128)(2,1)S(1)}, u32[]{:S(2)}, u32[]{:S(2)}) collective-permute-start(bf16[2816,128]{1,0:T(8,128)(2,1)S(1)} %collective-permute-done.9), channel_id=1, source_target_pairs={{0,30},{2,0},{4,2},{6,4},{8,6},{10,8},{12,10},{14,12},{16,14},{18,... | collective-permute-start | bytes 2162696 | tf_op jit(solution)/shard_map/ppermute | solution.py:199
  644.7 17.4 %collective-permute-start.12 = (bf16[2816,128]{1,0:T(8,128)(2,1)S(1)}, bf16[2816,128]{1,0:T(8,128)(2,1)S(1)}, u32[]{:S(2)}, u32[]{:S(2)}) collective-permute-start(bf16[2816,128]{1,0:T(8,128)(2,1)S(1)} %collective-permute-done.10), channel_id=1, source_target_pairs={{0,2},{2,4},{4,6},{6,8},{8,10},{10,12},{12,14},{14,16},{16,18},{18... | collective-permute-start | bytes 2162696 | tf_op jit(solution)/shard_map/ppermute | solution.py:192
  649.1 30.4 %collective-permute-start.13 = (bf16[2816,128]{1,0:T(8,128)(2,1)S(1)}, bf16[2816,128]{1,0:T(8,128)(2,1)S(1)}, u32[]{:S(2)}, u32[]{:S(2)}) collective-permute-start(bf16[2816,128]{1,0:T(8,128)(2,1)S(1)} %collective-permute-done.11), channel_id=1, source_target_pairs={{0,30},{2,0},{4,2},{6,4},{8,6},{10,8},{12,10},{14,12},{16,14},{18,... | collective-permute-start | bytes 2162696 | tf_op jit(solution)/shard_map/ppermute | solution.py:199
  662.0 30.9 %collective-permute-start.14 = (bf16[2816,128]{1,0:T(8,128)(2,1)S(1)}, bf16[2816,128]{1,0:T(8,128)(2,1)S(1)}, u32[]{:S(2)}, u32[]{:S(2)}) collective-permute-start(bf16[2816,128]{1,0:T(8,128)(2,1)S(1)} %collective-permute-done.12), channel_id=1, source_target_pairs={{0,2},{2,4},{4,6},{6,8},{8,10},{10,12},{12,14},{14,16},{16,18},{18... | collective-permute-start | bytes 2162696 | tf_op jit(solution)/shard_map/ppermute | solution.py:192
  (39 other events, 703.1 us)
Sparse Core Ops, SparseCore 0:
  369.6 7.3 reduce-scatter.2
  381.4 11.8 all-gather.7
  396.0 235.5 all-gather.9
  634.3 180.4 all-gather.11
  838.2 7.9 reduce-scatter.4
